TPU v7x, 32 devices: a whole 2x2x4 slice. The times are simulated.
32 devices in a mesh: ep: 16 (over z, y, x), tp: 2 (over core).
Axes of the slice: x: 2, y: 2, z: 4, core: 2. Of those that a mesh axis runs over, the one named last changes fastest.
Arguments:
- tokens: bfloat16 [256, 2048], P('ep'), may hold values from -6 to 6
- norm_gain: float32 [2048], replicated, may hold values from 0.1 to 1.9
- query_weight: bfloat16 [2048, 1024], P('ep', 'tp'), may hold values from -0.125 to 0.125
- key_weight: bfloat16 [2048, 1024], P('ep', 'tp'), may hold values from -0.125 to 0.125
- value_weight: bfloat16 [2048, 1024], P('ep', 'tp'), may hold values from -0.125 to 0.125
- outgate_weight: bfloat16 [2048, 1024], P('ep', 'tp'), may hold values from -0.125 to 0.125
- input_weight: bfloat16 [2048, 8], P('ep', 'tp'), may hold values from -0.125 to 0.125
- forget_weight: bfloat16 [2048, 8], P('ep', 'tp'), may hold values from -0.125 to 0.125
- forget_bias: float32 [8], P('tp'), may hold values from -1 to 5
- memory: float32 [256, 8, 128, 128], P('ep', 'tp'), may hold values from -2.4 to 2.4
- stabilizer: float32 [256, 8], P('ep', 'tp'), may hold values from -3 to 3
- head_gain: float32 [1024], P('tp'), may hold values from 0.1 to 1.9
- mix_weight: bfloat16 [1024, 2048], P('tp', 'ep'), may hold values from -0.1875 to 0.1875
- second_gain: float32 [2048], replicated, may hold values from 0.1 to 1.9
- route_experts: int32 [256, 4], P('ep'), may hold values from 0 to 15, all different within a row; in each aligned block of 16 rows (0 to 15, 16 to 31, ...) at most 8 rows name the same one
- route_weight: float32 [256, 4], P('ep'), may hold values from 0.1 to 1
- expert_gate: bfloat16 [16, 2048, 2048], P('ep', None, 'tp'), may hold values from -0.5 to 0.5
- expert_up: bfloat16 [16, 2048, 2048], P('ep', None, 'tp'), may hold values from -0.5 to 0.5
- expert_down: bfloat16 [16, 2048, 2048], P('ep', 'tp'), may hold values from -0.03125 to 0.03125
- dense_gate: bfloat16 [4096, 2048], P(('ep', 'tp')), may hold values from -0.125 to 0.125
- dense_up: bfloat16 [4096, 2048], P(('ep', 'tp')), may hold values from -0.125 to 0.125
- dense_down: bfloat16 [4096, 2048], P(('ep', 'tp')), may hold values from -0.09375 to 0.09375
- branch_scale: float32 [2048], replicated, may hold values from 0.3 to 1.5
Outputs:
- mixed: bfloat16 [256, 2048], P('ep', 'tp')
- memory_new: float32 [256, 8, 128, 128], P('ep', 'tp')
- stabilizer_new: float32 [256, 8], P('ep', 'tp')
Inputs may be any that keep to these rules, and one draw needn't show every extreme that they name: `route_experts`: each row names 4 different experts. Within each aligned block of 16 rows no expert is named by more than 8 rows, and in every draw some expert is named by exactly 8 rows of some block.
All inputs are finite; a program needn't handle non-finite values.
Results may differ from a plain program's by a relative error of at most 0.03.
Values may be sent and summed in bfloat16 or wider, within the bound.
A program may use at most 128 MiB of HBM per device.

v0:
```python
import jax
import jax.numpy as jnp
from jax import lax
from jax.sharding import PartitionSpec as P

norm_eps = 1e-05
clamp_limit = 7.0
sigmoid_slope = 1.702


def rms_scale(values, gain):
    mean_square = jnp.mean(values * values, axis=-1, keepdims=True)
    return values * lax.rsqrt(mean_square + norm_eps) * gain


def round_half(values):
    return lax.optimization_barrier(values.astype(jnp.bfloat16)).astype(jnp.float32)


def clamped_unit(gate_pre, up_pre):
    gate_clamped = jnp.minimum(gate_pre, clamp_limit)
    up_clamped = jnp.clip(up_pre, -clamp_limit, clamp_limit)
    return (
        (up_clamped + 1.0) * gate_clamped * jax.nn.sigmoid(sigmoid_slope * gate_clamped)
    ).astype(jnp.bfloat16)


def memory_step(projected, forget_bias, memory, stabilizer, head_gain):
    query_rows, key_rows, value_rows, outgate_rows, input_pre, forget_pre = projected
    sequences, head_count = stabilizer.shape
    head_size = memory.shape[-1]
    log_forget = jax.nn.log_sigmoid(forget_pre + forget_bias)
    stab_new = jnp.maximum(log_forget + stabilizer, input_pre)
    carried = jnp.exp(log_forget + stabilizer - stab_new)
    written = jnp.exp(input_pre - stab_new)
    query_heads = query_rows.astype(jnp.float32).reshape(sequences, head_count, head_size)
    key_heads = key_rows.astype(jnp.float32).reshape(
        sequences, head_count, head_size
    ) * head_size ** (-0.5)
    value_heads = value_rows.astype(jnp.float32).reshape(sequences, head_count, head_size)
    memory_new = (
        carried[:, :, None, None] * memory
        + written[:, :, None, None] * value_heads[:, :, :, None] * key_heads[:, :, None, :]
    )
    readout = jnp.einsum("bhvk,bhk->bhv", memory_new, query_heads, precision=lax.Precision.HIGHEST)
    out_gate = jax.nn.sigmoid(
        outgate_rows.astype(jnp.float32).reshape(sequences, head_count, head_size)
    )
    gated = (rms_scale(readout, head_gain.reshape(head_count, head_size)) * out_gate).astype(
        jnp.bfloat16
    )
    return (gated.reshape(sequences, head_count * head_size), memory_new, stab_new)


def expert_apply(rows, gate_weight, up_weight, down_weight):
    gate_pre = jnp.dot(rows, gate_weight, preferred_element_type=jnp.float32)
    up_pre = jnp.dot(rows, up_weight, preferred_element_type=jnp.float32)
    activity = clamped_unit(gate_pre, up_pre)
    return jnp.dot(activity, down_weight, preferred_element_type=jnp.float32).astype(jnp.bfloat16)


def slot_table(hit_mask, capacity):
    ranks = jnp.cumsum(hit_mask, axis=1) - 1.0
    slots = jnp.arange(capacity).astype(jnp.float32)
    return hit_mask[:, None, :] * (ranks[:, None, :] == slots[None, :, None]).astype(jnp.float32)


def body(
    tokens,
    norm_gain,
    query_weight,
    key_weight,
    value_weight,
    outgate_weight,
    input_weight,
    forget_weight,
    forget_bias,
    memory,
    stabilizer,
    head_gain,
    mix_weight,
    second_gain,
    route_experts,
    route_weight,
    expert_gate,
    expert_up,
    expert_down,
    dense_gate,
    dense_up,
    dense_down,
    branch_scale,
):
    sequences, model_width = tokens.shape
    ep_count = lax.axis_size("ep")
    tp_count = lax.axis_size("tp")
    part_width = model_width // tp_count
    top_count = route_experts.shape[1]
    expert_count = expert_gate.shape[0] * ep_count
    capacity = max(2, 2 * sequences * top_count // expert_count)
    inputs_float = tokens.astype(jnp.float32)
    normed = rms_scale(inputs_float, norm_gain).astype(jnp.bfloat16)
    weight_list = (
        query_weight,
        key_weight,
        value_weight,
        outgate_weight,
        input_weight,
        forget_weight,
    )
    columns = lax.all_to_all(normed, "ep", split_axis=1, concat_axis=0, tiled=True)
    joined = jnp.concatenate(weight_list, axis=1)
    summed_rows = lax.psum_scatter(
        jnp.dot(columns, joined, preferred_element_type=jnp.float32),
        "ep",
        scatter_dimension=0,
        tiled=True,
    )
    pieces = []
    lower = 0
    for weight in weight_list:
        pieces.append(summed_rows[:, lower : lower + weight.shape[1]])
        lower = lower + weight.shape[1]
    sums = tuple(pieces)
    projected = (
        sums[0].astype(jnp.bfloat16),
        sums[1].astype(jnp.bfloat16),
        sums[2].astype(jnp.bfloat16),
        sums[3].astype(jnp.bfloat16),
        sums[4],
        sums[5],
    )
    gated, memory_new, stab_new = memory_step(projected, forget_bias, memory, stabilizer, head_gain)
    partial_value = jnp.dot(
        gated,
        lax.all_gather(mix_weight, "ep", axis=1, tiled=True),
        preferred_element_type=jnp.float32,
    )
    attended = lax.psum(round_half(partial_value).astype(jnp.bfloat16), "tp").astype(jnp.float32)
    residual = (inputs_float + attended).astype(jnp.bfloat16)
    residual_float = residual.astype(jnp.float32)
    normed_second = rms_scale(residual_float, second_gain).astype(jnp.bfloat16)
    own_residual = lax.dynamic_slice_in_dim(
        residual_float, lax.axis_index("tp") * part_width, part_width, 1
    )
    matched = route_experts[:, :, None] == jnp.arange(expert_count)[None, None, :]
    hit_mask = jnp.any(matched, axis=1).astype(jnp.float32).T
    weights = jnp.sum(jnp.where(matched, route_weight[:, :, None], 0.0), axis=1).T
    select = slot_table(hit_mask, capacity)
    outgoing = jnp.einsum(
        "ecs,sd->ecd",
        select.astype(jnp.bfloat16),
        normed_second,
        preferred_element_type=jnp.float32,
    ).astype(jnp.bfloat16)
    received = lax.all_to_all(outgoing, "ep", split_axis=0, concat_axis=0, tiled=True)
    count = received.shape[1]
    partial_out = expert_apply(
        received.reshape(-1, model_width), expert_gate[0], expert_up[0], expert_down[0]
    )
    halves = lax.psum_scatter(
        partial_out.astype(jnp.float32).astype(jnp.bfloat16), "tp", scatter_dimension=1, tiled=True
    ).astype(jnp.float32)
    returned = lax.all_to_all(
        halves.reshape(ep_count, count, part_width).astype(jnp.bfloat16),
        "ep",
        split_axis=0,
        concat_axis=0,
        tiled=True,
    ).astype(jnp.float32)
    routed = jnp.einsum(
        "ecs,ecd->sd", select * weights[:, None, :], returned, precision=lax.Precision.HIGHEST
    )
    all_rows = lax.all_gather(normed_second, "ep", axis=0, tiled=True)
    gate_rows = jnp.einsum("fd,td->ft", dense_gate, all_rows, preferred_element_type=jnp.float32)
    lift_rows = jnp.einsum("fd,td->ft", dense_up, all_rows, preferred_element_type=jnp.float32)
    activity = (
        (jax.nn.silu(gate_rows) * lift_rows).astype(jnp.bfloat16).reshape(-1, ep_count, sequences)
    )
    down_parts = dense_down.reshape(-1, tp_count, part_width)
    term = jnp.einsum("fjs,fhd->jhsd", activity, down_parts, preferred_element_type=jnp.float32)
    branch = lax.psum_scatter(
        (term * branch_scale.reshape(1, tp_count, 1, part_width)).reshape(-1, part_width),
        ("ep", "tp"),
        scatter_dimension=0,
        tiled=True,
    )
    mixed = own_residual + routed + branch
    return (mixed.astype(jnp.bfloat16), memory_new, stab_new)


def solution(mesh):
    in_specs = (
        P("ep", None),
        P(),
        P("ep", "tp"),
        P("ep", "tp"),
        P("ep", "tp"),
        P("ep", "tp"),
        P("ep", "tp"),
        P("ep", "tp"),
        P("tp"),
        P("ep", "tp", None, None),
        P("ep", "tp"),
        P("tp"),
        P("tp", "ep"),
        P(),
        P("ep", None),
        P("ep", None),
        P("ep", None, "tp"),
        P("ep", None, "tp"),
        P("ep", "tp", None),
        P(("ep", "tp"), None),
        P(("ep", "tp"), None),
        P(("ep", "tp"), None),
        P(),
    )
    out_specs = (P("ep", "tp"), P("ep", "tp", None, None), P("ep", "tp"))
    return jax.shard_map(body, mesh=mesh, in_specs=in_specs, out_specs=out_specs, check_vma=False)
```

profile of v0, /device:TPU:0, one launch (start us, length us, event | category | flops | bytes accessed | tf_op | source)
XLA Modules:
  0.0 416.8 jit_solution(380059310604357217)
XLA Ops:
  7.2 1.0 fusion.48
  8.2 1.6 copy_bitcast_fusion
  9.8 8.3 %all-to-all-start = ((bf16[16,16,128]{2,0,1:T(8,128)(2,1)}), bf16[16,16,128]{2,0,1:T(8,128)(2,1)S(1)}, u32[]{:S(2)}, u32[]{:S(2)}) async-start(bf16[16,16,128]{2,0,1:T(8,128)(2,1)} %copy_bitcast_fusion), calls=%async_computation | async-start | bytes 131072 | tf_op jit(solution)/shard_map/all_to_all | solution.py:110
  18.2 0.8 copy.62
  19.8 1.2 concatenate.3
  21.0 4.7 %all-to-all-done = bf16[16,16,128]{2,0,1:T(8,128)(2,1)S(1)} async-done(((bf16[16,16,128]{2,0,1:T(8,128)(2,1)}), bf16[16,16,128]{2,0,1:T(8,128)(2,1)S(1)}, u32[]{:S(2)}, u32[]{:S(2)}) %all-to-all-start) | async-done | bytes 65568 | tf_op jit(solution)/shard_map/all_to_all | solution.py:110
  25.7 1.8 fusion.72
  28.8 77.2 %reduce-scatter.4.cloned.1.call-done = f32[16,2056]{1,0:T(8,128)} async-done(((f32[256,2056]{1,0:T(8,128)}), f32[16,2056]{1,0:T(8,128)}) %reduce-scatter.4.cloned.1.call-update) | async-done | bytes 131600 | tf_op jit(solution)/shard_map/reduce_scatter | solution.py:112
  106.0 0.9 convert.8
  107.1 0.9 subtract_exponential_fusion.1
  108.8 3.0 multiply_add_fusion
  111.8 2.0 copy-done.1
  113.8 3.3 fusion.73
  117.4 51.6 %all-gather.3.cloned.1.call-done = bf16[512,2048]{1,0:T(8,128)(2,1)} async-done(((bf16[512,128]{1,0:T(8,128)(2,1)}), bf16[512,2048]{1,0:T(8,128)(2,1)}) %all-gather.3.cloned.1.call-update) | async-done | bytes 2097168 | tf_op jit(solution)/shard_map/all_gather | solution.py:135
  169.0 2.6 convolution_convert_fusion.1
  171.8 15.9 %all-reduce.2.cloned.1.call-done = bf16[16,2048]{1,0:T(8,128)(2,1)} async-done(((bf16[16,2048]{1,0:T(8,128)(2,1)}), bf16[16,2048]{1,0:T(8,128)(2,1)}) %all-reduce.2.cloned.1.call-update) | async-done | bytes 65552 | tf_op jit(solution)/shard_map/psum | solution.py:138
  187.7 1.0 fusion.52
  188.7 0.9 multiply_convert_fusion
  189.7 1.1 convolution_convert_fusion
  190.7 6.8 %all-to-all-start.1 = ((bf16[16,8,2048]{2,1,0:T(8,128)(2,1)}), bf16[16,8,2048]{2,1,0:T(8,128)(2,1)S(1)}, u32[]{:S(2)}, u32[]{:S(2)}) async-start(bf16[16,8,2048]{2,1,0:T(8,128)(2,1)} %convolution_convert_fusion), calls=%async_computation.2 | async-start | bytes 1048576 | tf_op jit(solution)/shard_map/all_to_all | solution.py:155
  198.2 14.9 %all-to-all-done.1 = bf16[16,8,2048]{2,1,0:T(8,128)(2,1)S(1)} async-done(((bf16[16,8,2048]{2,1,0:T(8,128)(2,1)}), bf16[16,8,2048]{2,1,0:T(8,128)(2,1)S(1)}, u32[]{:S(2)}, u32[]{:S(2)}) %all-to-all-start.1) | async-done | bytes 524320 | tf_op jit(solution)/shard_map/all_to_all | solution.py:155
  213.1 2.9 fusion.12
  216.0 5.7 %fusion.6 = bf16[128,2048]{1,0:T(8,128)(2,1)} fusion(bf16[1,1024,2048]{2,1,0:T(8,128)(2,1)} %param.41, f32[128,1024]{1,0:T(8,128)S(1)} %fusion.12, bf16[1,2048,1024]{2,1,0:T(8,128)(2,1)} %param.40, bf16[16,8,2048]{2,1,0:T(8,128)(2,1)S(1)} %all-to-all-done.1), kind=kOutput, calls=%fused_computation.7 | convolution fusion | flops 1075183616 | bytes 9961472 | tf_op jit(solution)/shard_map/dot_general | solution.py:59
  221.9 35.4 %all-gather.5.cloned.1.call-done = bf16[256,2048]{1,0:T(8,128)(2,1)} async-done(((bf16[16,2048]{1,0:T(8,128)(2,1)}), bf16[256,2048]{1,0:T(8,128)(2,1)}) %all-gather.5.cloned.1.call-update) | async-done | bytes 1048592 | tf_op jit(solution)/shard_map/all_gather | solution.py:173
  257.3 1.7 convolution_bitcast_fusion.1
  258.9 1.7 fusion.28
  260.6 1.8 convolution_multiply_fusion
  262.4 3.8 reduce-scatter.6.cloned.1.call-done
  266.2 6.7 %all-to-all-start.2 = ((bf16[16,8,1024]{2,1,0:T(8,128)(2,1)}), bf16[16,8,1024]{2,1,0:T(8,128)(2,1)S(1)}, u32[]{:S(2)}, u32[]{:S(2)}) async-start(bf16[16,8,1024]{2,1,0:T(8,128)(2,1)} %bitcast.100), calls=%async_computation.4 | async-start | bytes 524288 | tf_op jit(solution)/shard_map/all_to_all | solution.py:163
  273.6 10.3 %all-to-all-done.2 = bf16[16,8,1024]{2,1,0:T(8,128)(2,1)S(1)} async-done(((bf16[16,8,1024]{2,1,0:T(8,128)(2,1)}), bf16[16,8,1024]{2,1,0:T(8,128)(2,1)S(1)}, u32[]{:S(2)}, u32[]{:S(2)}) %all-to-all-start.2) | async-done | bytes 262176 | tf_op jit(solution)/shard_map/all_to_all | solution.py:163
  284.0 124.0 %reduce-scatter.8.cloned.1.call-done = f32[16,1024]{1,0:T(8,128)} async-done(((f32[512,1024]{1,0:T(8,128)}), f32[16,1024]{1,0:T(8,128)}) %reduce-scatter.8.cloned.1.call-update) | async-done | bytes 65552 | tf_op jit(solution)/shard_map/reduce_scatter | solution.py:181
  407.9 2.0 fusion.31
  (64 shorter events, 4.9 us)
Async XLA Ops:
  7.2 250.1 %copy-start = (bf16[128,2048]{1,0:T(8,128)(2,1)S(1)}, bf16[128,2048]{1,0:T(8,128)(2,1)}, u32[]{:S(2)}) copy-start(bf16[128,2048]{1,0:T(8,128)(2,1)} %param.42) | copy-start | bytes 1572868
  7.2 21.1 %copy-start.8 = (f32[16,4]{0,1:T(4,128)S(1)}, f32[16,4]{0,1:T(4,128)}, u32[]{:S(2)}) copy-start(f32[16,4]{0,1:T(4,128)} %param.33) | copy-start | bytes 772
  7.2 21.2 %copy-start.7 = (s32[16,4]{0,1:T(4,128)S(1)}, s32[16,4]{0,1:T(4,128)}, u32[]{:S(2)}) copy-start(s32[16,4]{0,1:T(4,128)} %param.37) | copy-start | bytes 772
  7.2 99.9 %copy-start.11 = (f32[4]{0:T(128)S(1)}, f32[4]{0:T(128)}, u32[]{:S(2)}) copy-start(f32[4]{0:T(128)} %param.31) | copy-start | bytes 52
  9.8 15.9 %all-to-all-start = ((bf16[16,16,128]{2,0,1:T(8,128)(2,1)}), bf16[16,16,128]{2,0,1:T(8,128)(2,1)S(1)}, u32[]{:S(2)}, u32[]{:S(2)}) async-start(bf16[16,16,128]{2,0,1:T(8,128)(2,1)} %copy_bitcast_fusion), calls=%async_computation | async-start | bytes 131072 | tf_op jit(solution)/shard_map/all_to_all | solution.py:110
  18.2 87.9 %reduce-scatter.4.cloned.1.call-start = ((), (), s32[]{:S(2)}) async-start(), calls=%async_computation.6 | async-start | bytes 2367488 | tf_op jit(solution)/shard_map/reduce_scatter | solution.py:112
  27.5 141.5 %all-gather.3.cloned.1.call-start = ((), (), s32[]{:S(2)}) async-start(), calls=%async_computation.7 | async-start | bytes 2228224 | tf_op jit(solution)/shard_map/all_gather | solution.py:135
  28.3 159.5 %all-reduce.2.cloned.1.call-start = ((), (), s32[]{:S(2)}) async-start(), calls=%async_computation.8 | async-start | bytes 131072 | tf_op jit(solution)/shard_map/psum | solution.py:138
  111.8 2.0 copy-start.1
  113.8 3.5 copy-start.9
  113.8 73.9 %copy-start.2 = (bf16[16,2048]{1,0:T(8,128)(2,1)S(1)}, bf16[16,2048]{1,0:T(8,128)(2,1)}, u32[]{:S(2)}) copy-start(bf16[16,2048]{1,0:T(8,128)(2,1)} %param.23) | copy-start | bytes 196612
  113.8 74.9 %copy-start.5 = (f32[2048]{0:T(1024)S(1)}, f32[2048]{0:T(1024)}, u32[]{:S(2)}) copy-start(f32[2048]{0:T(1024)} %param.36) | copy-start | bytes 24580
  189.6 8.0 %copy-start.3 = (bf16[16,2048]{1,0:T(8,128)(2,1)}, bf16[16,2048]{1,0:T(8,128)(2,1)S(1)}, u32[]{:S(2)}) copy-start(bf16[16,2048]{1,0:T(8,128)(2,1)S(1)} %multiply_convert_fusion) | copy-start | bytes 196612
  190.7 22.3 %all-to-all-start.1 = ((bf16[16,8,2048]{2,1,0:T(8,128)(2,1)}), bf16[16,8,2048]{2,1,0:T(8,128)(2,1)S(1)}, u32[]{:S(2)}, u32[]{:S(2)}) async-start(bf16[16,8,2048]{2,1,0:T(8,128)(2,1)} %convolution_convert_fusion), calls=%async_computation.2 | async-start | bytes 1048576 | tf_op jit(solution)/shard_map/all_to_all | solution.py:155
  197.6 59.7 %all-gather.5.cloned.1.call-start = ((), (), s32[]{:S(2)}) async-start(), calls=%async_computation.10 | async-start | bytes 1114112 | tf_op jit(solution)/shard_map/all_gather | solution.py:173
  198.2 68.0 %reduce-scatter.6.cloned.1.call-start = ((), (), s32[]{:S(2)}) async-start(), calls=%async_computation.9 | async-start | bytes 786432 | tf_op jit(solution)/shard_map/reduce_scatter | solution.py:160
  216.0 5.8 %copy-start.6 = (f32[2048]{0:T(1024)S(1)}, f32[2048]{0:T(1024)}, u32[]{:S(2)}) copy-start(f32[2048]{0:T(1024)} %param.45) | copy-start | bytes 24580
  216.0 43.0 %copy-start.12 = (bf16[128,2048]{1,0:T(8,128)(2,1)S(1)}, bf16[128,2048]{1,0:T(8,128)(2,1)}, u32[]{:S(2)}) copy-start(bf16[128,2048]{1,0:T(8,128)(2,1)} %param.43) | copy-start | bytes 1572868
  221.7 38.9 %copy-start.4 = (bf16[128,2048]{1,0:T(8,128)(2,1)S(1)}, bf16[128,2048]{1,0:T(8,128)(2,1)}, u32[]{:S(2)}) copy-start(bf16[128,2048]{1,0:T(8,128)(2,1)} %param.44) | copy-start | bytes 1572868
  221.8 186.2 %reduce-scatter.8.cloned.1.call-start = ((), (), s32[]{:S(2)}) async-start(), calls=%async_computation.11 | async-start | bytes 2162688 | tf_op jit(solution)/shard_map/reduce_scatter | solution.py:181
  221.8 51.1 %copy-start.10 = (f32[16,4]{0,1:T(4,128)S(1)}, f32[16,4]{0,1:T(4,128)}, u32[]{:S(2)}) copy-start(f32[16,4]{0,1:T(4,128)} %param.38) | copy-start | bytes 772
  266.2 17.8 %all-to-all-start.2 = ((bf16[16,8,1024]{2,1,0:T(8,128)(2,1)}), bf16[16,8,1024]{2,1,0:T(8,128)(2,1)S(1)}, u32[]{:S(2)}, u32[]{:S(2)}) async-start(bf16[16,8,1024]{2,1,0:T(8,128)(2,1)} %bitcast.100), calls=%async_computation.4 | async-start | bytes 524288 | tf_op jit(solution)/shard_map/all_to_all | solution.py:163
Sparse Core Ops, SparseCore 0:
  27.6 78.3 reduce-scatter.3
  108.7 60.2 all-gather.2
  171.8 15.9 all-reduce.1
  200.8 56.3 all-gather.4
  259.4 6.7 reduce-scatter.5
  268.3 139.6 reduce-scatter.7
where the time goes:
time: 418 us; the launch traced here: 417 us
  waiting for transfers between devices  339 us (81%)
  matrix products  24.5 us (6%)
  starting transfers between devices  22.1 us (5%)
  between operations  14.4 us (3%)
  other arithmetic  10.8 us (3%)
  local copies, waits for them, and re-layouts  5.91 us (1%)
    reduce_scatter x1, waiting for transfers between devices, body(): lax.psum_scatter((term * branch_scale.reshape(1, tp_count, 1, part_width)...  124 us
    reduce_scatter x1, waiting for transfers between devices, body(): lax.psum_scatter(jnp.dot(columns, joined, preferred_element_type=jnp.floa...  77.2 us
    all_gather x1, waiting for transfers between devices, body(): lax.all_gather(mix_weight, 'ep', axis=1, tiled=True)  51.6 us
    all_gather x1, waiting for transfers between devices, body(): all_rows = lax.all_gather(normed_second, 'ep', axis=0, tiled=True)  35.4 us
    psum x1, waiting for transfers between devices, body(): lax.psum(round_half(partial_value).astype(jnp.bfloat16), 'tp')  15.9 us
    all_to_all x1, waiting for transfers between devices, body(): lax.all_to_all(outgoing, 'ep', split_axis=0, concat_axis=0, tiled=True)  14.9 us
    all_to_all x1, waiting for transfers between devices, body(): lax.all_to_all(halves.reshape(ep_count, count, part_width).astype(jnp.bfl...  10.3 us
  transfers between devices with their start and end apart: 9, of which 9 were waited for; matrix products, arithmetic and copies ran while one was open for 7% of the time, Pallas kernels for 0%

commit v1 on v0

--- a/solution.py
+++ b/solution.py
@@ -170,7 +170,22 @@
     routed = jnp.einsum(
         "ecs,ecd->sd", select * weights[:, None, :], returned, precision=lax.Precision.HIGHEST
     )
-    all_rows = lax.all_gather(normed_second, "ep", axis=0, tiled=True)
+    ways, here, step = (lax.axis_size("ep"), lax.axis_index("ep"), normed_second.shape[0])
+    shape = [n * ways if d == 0 else n for d, n in enumerate(normed_second.shape)]
+    all_rows = lax.dynamic_update_slice_in_dim(
+        jnp.zeros(shape, normed_second.dtype), normed_second, here * step, axis=0
+    )
+    going_up = going_down = normed_second
+    for far in range(1, ways // 2 + 1):
+        going_up = lax.ppermute(going_up, "ep", [(d, (d + 1) % ways) for d in range(ways)])
+        all_rows = lax.dynamic_update_slice_in_dim(
+            all_rows, going_up, (here - far) % ways * step, axis=0
+        )
+        if 2 * far < ways:
+            going_down = lax.ppermute(going_down, "ep", [(d, (d - 1) % ways) for d in range(ways)])
+            all_rows = lax.dynamic_update_slice_in_dim(
+                all_rows, going_down, (here + far) % ways * step, axis=0
+            )
     gate_rows = jnp.einsum("fd,td->ft", dense_gate, all_rows, preferred_element_type=jnp.float32)
     lift_rows = jnp.einsum("fd,td->ft", dense_up, all_rows, preferred_element_type=jnp.float32)
     activity = (

time: 418 us -> 426 us (1.019)
  starting transfers between devices: 22.1 us -> 58.3 us
  waiting for transfers between devices: 339 us -> 313 us
    ppermute x0 -> x15, starting transfers between devices: none -> 39.5 us  [the longest x7 35.8 us: body(): lax.ppermute(going_down, 'ep', [(d, (d - 1) % ways) for d in range(ways)])]
    all_gather x1 -> x0, waiting for transfers between devices: 35.4 us -> none  [body(): all_rows = lax.all_gather(normed_second, 'ep', axis=0, tiled=True)]
    ppermute x0 -> x15, waiting for transfers between devices: none -> 21.9 us  [the longest x8 21.9 us: body(): lax.ppermute(going_up, 'ep', [(d, (d + 1) % ways) for d in range(ways)])]
    all_to_all x1, waiting for transfers between devices: 14.9 us -> 0.01 us  [body(): lax.all_to_all(outgoing, 'ep', split_axis=0, concat_axis=0, tiled=True)]
  transfers between devices with their start and end apart: 9 -> 23, of which waited for: 9 -> 13; matrix products, arithmetic and copies ran while one was open for 7% -> 6% of each run, Pallas kernels for 0% -> 0%
where the time goes in v1:
time: 426 us; the launch traced here: 425 us
  waiting for transfers between devices  313 us (73%)
  starting transfers between devices  58.3 us (14%)
  matrix products  22 us (5%)
  between operations  14.6 us (3%)
  other arithmetic  10.7 us (3%)
  local copies, waits for them, and re-layouts  6.18 us (1%)
    reduce_scatter x1, waiting for transfers between devices, body(): lax.psum_scatter((term * branch_scale.reshape(1, tp_count, 1, part_width)...  124 us
    reduce_scatter x1, waiting for transfers between devices, body(): lax.psum_scatter(jnp.dot(columns, joined, preferred_element_type=jnp.floa...  77.3 us
    all_gather x1, waiting for transfers between devices, body(): lax.all_gather(mix_weight, 'ep', axis=1, tiled=True)  51.6 us
    ppermute x7, starting transfers between devices, body(): lax.ppermute(going_down, 'ep', [(d, (d - 1) % ways) for d in range(ways)])  35.8 us
    ppermute x8, waiting for transfers between devices, body(): lax.ppermute(going_up, 'ep', [(d, (d + 1) % ways) for d in range(ways)])  21.9 us
    psum x1, waiting for transfers between devices, body(): lax.psum(round_half(partial_value).astype(jnp.bfloat16), 'tp')  15.5 us
    all_to_all x1, waiting for transfers between devices, body(): lax.all_to_all(halves.reshape(ep_count, count, part_width).astype(jnp.bfl...  10.3 us
  transfers between devices with their start and end apart: 23, of which 13 were waited for; matrix products, arithmetic and copies ran while one was open for 6% of the time, Pallas kernels for 0%

profile of v1, /device:TPU:0, one launch (start us, length us, event | category | flops | bytes accessed | tf_op | source)
XLA Modules:
  0.0 424.7 jit_solution(10314846912321315128)
XLA Ops:
  9.8 8.3 %all-to-all-start = ((bf16[16,16,128]{2,0,1:T(8,128)(2,1)}), bf16[16,16,128]{2,0,1:T(8,128)(2,1)S(1)}, u32[]{:S(2)}, u32[]{:S(2)}) async-start(bf16[16,16,128]{2,0,1:T(8,128)(2,1)} %copy_bitcast_fusion), calls=%async_computation | async-start | bytes 131072 | tf_op jit(solution)/shard_map/all_to_all | solution.py:110
  21.0 4.7 %all-to-all-done = bf16[16,16,128]{2,0,1:T(8,128)(2,1)S(1)} async-done(((bf16[16,16,128]{2,0,1:T(8,128)(2,1)}), bf16[16,16,128]{2,0,1:T(8,128)(2,1)S(1)}, u32[]{:S(2)}, u32[]{:S(2)}) %all-to-all-start) | async-done | bytes 65568 | tf_op jit(solution)/shard_map/all_to_all | solution.py:110
  28.8 77.3 %reduce-scatter.4.cloned.1.call-done = f32[16,2056]{1,0:T(8,128)} async-done(((f32[256,2056]{1,0:T(8,128)}), f32[16,2056]{1,0:T(8,128)}) %reduce-scatter.4.cloned.1.call-update) | async-done | bytes 131600 | tf_op jit(solution)/shard_map/reduce_scatter | solution.py:112
  108.9 3.0 multiply_add_fusion
  111.9 2.0 copy-done.1
  113.9 3.4 fusion.71
  117.5 51.6 %all-gather.2.cloned.1.call-done = bf16[512,2048]{1,0:T(8,128)(2,1)} async-done(((bf16[512,128]{1,0:T(8,128)(2,1)}), bf16[512,2048]{1,0:T(8,128)(2,1)}) %all-gather.2.cloned.1.call-update) | async-done | bytes 2097168 | tf_op jit(solution)/shard_map/all_gather | solution.py:135
  169.1 2.6 convolution_convert_fusion.1
  172.3 15.5 %all-reduce.2.cloned.1.call-done = bf16[16,2048]{1,0:T(8,128)(2,1)} async-done(((bf16[16,2048]{1,0:T(8,128)(2,1)}), bf16[16,2048]{1,0:T(8,128)(2,1)}) %all-reduce.2.cloned.1.call-update) | async-done | bytes 65552 | tf_op jit(solution)/shard_map/psum | solution.py:138
  189.9 1.8 collective-permute-start
  191.7 3.8 collective-permute-start.1
  196.6 3.6 all-to-all-start.1
  200.2 1.9 collective-permute-start.2
  202.1 3.8 collective-permute-start.3
  206.0 10.2 %collective-permute-done.2 = bf16[16,2048]{1,0:T(8,128)(2,1)S(1)} collective-permute-done((bf16[16,2048]{1,0:T(8,128)(2,1)S(1)}, bf16[16,2048]{1,0:T(8,128)(2,1)S(1)}, u32[]{:S(2)}, u32[]{:S(2)}) %collective-permute-start.2) | collective-permute-done | bytes 65568 | tf_op jit(solution)/shard_map/ppermute | solution.py:180
  216.2 5.6 %collective-permute-start.5 = (bf16[16,2048]{1,0:T(8,128)(2,1)S(1)}, bf16[16,2048]{1,0:T(8,128)(2,1)S(1)}, u32[]{:S(2)}, u32[]{:S(2)}) collective-permute-start(bf16[16,2048]{1,0:T(8,128)(2,1)S(1)} %collective-permute-done.3), channel_id=1, source_target_pairs={{0,30},{2,0},{4,2},{6,4},{8,6},{10,8},{12,10},{14,12},{16,14},{18,... | collective-permute-start | bytes 196616 | tf_op jit(solution)/shard_map/ppermute | solution.py:185
  221.9 2.2 collective-permute-done.4
  224.1 5.6 %collective-permute-start.7 = (bf16[16,2048]{1,0:T(8,128)(2,1)S(1)}, bf16[16,2048]{1,0:T(8,128)(2,1)S(1)}, u32[]{:S(2)}, u32[]{:S(2)}) collective-permute-start(bf16[16,2048]{1,0:T(8,128)(2,1)S(1)} %collective-permute-done.5), channel_id=1, source_target_pairs={{0,30},{2,0},{4,2},{6,4},{8,6},{10,8},{12,10},{14,12},{16,14},{18,... | collective-permute-start | bytes 196616 | tf_op jit(solution)/shard_map/ppermute | solution.py:185
  229.7 2.3 collective-permute-done.6
  232.0 5.6 %collective-permute-start.9 = (bf16[16,2048]{1,0:T(8,128)(2,1)S(1)}, bf16[16,2048]{1,0:T(8,128)(2,1)S(1)}, u32[]{:S(2)}, u32[]{:S(2)}) collective-permute-start(bf16[16,2048]{1,0:T(8,128)(2,1)S(1)} %collective-permute-done.7), channel_id=1, source_target_pairs={{0,30},{2,0},{4,2},{6,4},{8,6},{10,8},{12,10},{14,12},{16,14},{18,... | collective-permute-start | bytes 196616 | tf_op jit(solution)/shard_map/ppermute | solution.py:185
  237.7 2.2 collective-permute-done.8
  239.9 5.6 %collective-permute-start.11 = (bf16[16,2048]{1,0:T(8,128)(2,1)S(1)}, bf16[16,2048]{1,0:T(8,128)(2,1)S(1)}, u32[]{:S(2)}, u32[]{:S(2)}) collective-permute-start(bf16[16,2048]{1,0:T(8,128)(2,1)S(1)} %collective-permute-done.9), channel_id=1, source_target_pairs={{0,30},{2,0},{4,2},{6,4},{8,6},{10,8},{12,10},{14,12},{16,14},{18,... | collective-permute-start | bytes 196616 | tf_op jit(solution)/shard_map/ppermute | solution.py:185
  245.5 2.2 collective-permute-done.10
  247.8 5.6 %collective-permute-start.13 = (bf16[16,2048]{1,0:T(8,128)(2,1)S(1)}, bf16[16,2048]{1,0:T(8,128)(2,1)S(1)}, u32[]{:S(2)}, u32[]{:S(2)}) collective-permute-start(bf16[16,2048]{1,0:T(8,128)(2,1)S(1)} %collective-permute-done.11), channel_id=1, source_target_pairs={{0,30},{2,0},{4,2},{6,4},{8,6},{10,8},{12,10},{14,12},{16,14},{18,... | collective-permute-start | bytes 196616 | tf_op jit(solution)/shard_map/ppermute | solution.py:185
  253.4 2.7 collective-permute-done.12
  256.2 2.9 fusion.12
  259.1 5.7 %fusion.6 = bf16[128,2048]{1,0:T(8,128)(2,1)} fusion(bf16[1,1024,2048]{2,1,0:T(8,128)(2,1)} %param.41, f32[128,1024]{1,0:T(8,128)S(1)} %fusion.12, bf16[1,2048,1024]{2,1,0:T(8,128)(2,1)} %param.40, bf16[16,8,2048]{2,1,0:T(8,128)(2,1)S(1)} %all-to-all-done.1), kind=kOutput, calls=%fused_computation.7 | convolution fusion | flops 1075183616 | bytes 9961472 | tf_op jit(solution)/shard_map/dot_general | solution.py:59
  267.6 6.7 %reduce-scatter.6.cloned.1.call-done = bf16[128,1024]{1,0:T(8,128)(2,1)} async-done(((bf16[128,2048]{1,0:T(8,128)(2,1)}), bf16[128,1024]{1,0:T(8,128)(2,1)}) %reduce-scatter.6.cloned.1.call-update) | async-done | bytes 262160 | tf_op jit(solution)/shard_map/reduce_scatter | solution.py:160
  274.3 6.7 %all-to-all-start.2 = ((bf16[16,8,1024]{2,1,0:T(8,128)(2,1)}), bf16[16,8,1024]{2,1,0:T(8,128)(2,1)S(1)}, u32[]{:S(2)}, u32[]{:S(2)}) async-start(bf16[16,8,1024]{2,1,0:T(8,128)(2,1)} %bitcast.96), calls=%async_computation.4 | async-start | bytes 524288 | tf_op jit(solution)/shard_map/all_to_all | solution.py:163
  281.8 10.3 %all-to-all-done.2 = bf16[16,8,1024]{2,1,0:T(8,128)(2,1)S(1)} async-done(((bf16[16,8,1024]{2,1,0:T(8,128)(2,1)}), bf16[16,8,1024]{2,1,0:T(8,128)(2,1)S(1)}, u32[]{:S(2)}, u32[]{:S(2)}) %all-to-all-start.2) | async-done | bytes 262176 | tf_op jit(solution)/shard_map/all_to_all | solution.py:163
  292.1 124.1 %reduce-scatter.8.cloned.1.call-done = f32[16,1024]{1,0:T(8,128)} async-done(((f32[512,1024]{1,0:T(8,128)}), f32[16,1024]{1,0:T(8,128)}) %reduce-scatter.8.cloned.1.call-update) | async-done | bytes 65552 | tf_op jit(solution)/shard_map/reduce_scatter | solution.py:196
  416.2 2.0 fusion.29
  (105 shorter events, 18.4 us)
Async XLA Ops:
  7.2 257.8 %copy-start = (bf16[128,2048]{1,0:T(8,128)(2,1)S(1)}, bf16[128,2048]{1,0:T(8,128)(2,1)}, u32[]{:S(2)}) copy-start(bf16[128,2048]{1,0:T(8,128)(2,1)} %param.42) | copy-start | bytes 1572868
  7.2 21.1 %copy-start.7 = (f32[16,4]{0,1:T(4,128)S(1)}, f32[16,4]{0,1:T(4,128)}, u32[]{:S(2)}) copy-start(f32[16,4]{0,1:T(4,128)} %param.33) | copy-start | bytes 772
  7.2 21.2 %copy-start.6 = (s32[16,4]{0,1:T(4,128)S(1)}, s32[16,4]{0,1:T(4,128)}, u32[]{:S(2)}) copy-start(s32[16,4]{0,1:T(4,128)} %param.37) | copy-start | bytes 772
  7.2 100.0 %copy-start.10 = (f32[4]{0:T(128)S(1)}, f32[4]{0:T(128)}, u32[]{:S(2)}) copy-start(f32[4]{0:T(128)} %param.31) | copy-start | bytes 52
  9.8 15.9 %all-to-all-start = ((bf16[16,16,128]{2,0,1:T(8,128)(2,1)}), bf16[16,16,128]{2,0,1:T(8,128)(2,1)S(1)}, u32[]{:S(2)}, u32[]{:S(2)}) async-start(bf16[16,16,128]{2,0,1:T(8,128)(2,1)} %copy_bitcast_fusion), calls=%async_computation | async-start | bytes 131072 | tf_op jit(solution)/shard_map/all_to_all | solution.py:110
  18.2 88.0 %reduce-scatter.4.cloned.1.call-start = ((), (), s32[]{:S(2)}) async-start(), calls=%async_computation.6 | async-start | bytes 2367488 | tf_op jit(solution)/shard_map/reduce_scatter | solution.py:112
  27.5 141.6 %all-gather.2.cloned.1.call-start = ((), (), s32[]{:S(2)}) async-start(), calls=%async_computation.7 | async-start | bytes 2228224 | tf_op jit(solution)/shard_map/all_gather | solution.py:135
  28.3 159.5 %all-reduce.2.cloned.1.call-start = ((), (), s32[]{:S(2)}) async-start(), calls=%async_computation.8 | async-start | bytes 131072 | tf_op jit(solution)/shard_map/psum | solution.py:138
  113.9 58.2 %copy-start.5 = (f32[2048]{0:T(1024)S(1)}, f32[2048]{0:T(1024)}, u32[]{:S(2)}) copy-start(f32[2048]{0:T(1024)} %param.45) | copy-start | bytes 24580
  113.9 73.9 %copy-start.2 = (bf16[16,2048]{1,0:T(8,128)(2,1)S(1)}, bf16[16,2048]{1,0:T(8,128)(2,1)}, u32[]{:S(2)}) copy-start(bf16[16,2048]{1,0:T(8,128)(2,1)} %param.23) | copy-start | bytes 196612
  113.9 75.0 %copy-start.4 = (f32[2048]{0:T(1024)S(1)}, f32[2048]{0:T(1024)}, u32[]{:S(2)}) copy-start(f32[2048]{0:T(1024)} %param.36) | copy-start | bytes 24580
  189.9 10.4 %collective-permute-start = (bf16[16,2048]{1,0:T(8,128)(2,1)S(1)}, bf16[16,2048]{1,0:T(8,128)(2,1)S(1)}, u32[]{:S(2)}, u32[]{:S(2)}) collective-permute-start(bf16[16,2048]{1,0:T(8,128)(2,1)S(1)} %get-tuple-element.16), channel_id=1, source_target_pairs={{0,2},{2,4},{4,6},{6,8},{8,10},{10,12},{12,14},{14,16},{16,18},{18... | collective-permute-start | bytes 196616 | tf_op jit(solution)/shard_map/ppermute | solution.py:180
  191.7 10.4 %collective-permute-start.1 = (bf16[16,2048]{1,0:T(8,128)(2,1)S(1)}, bf16[16,2048]{1,0:T(8,128)(2,1)S(1)}, u32[]{:S(2)}, u32[]{:S(2)}) collective-permute-start(bf16[16,2048]{1,0:T(8,128)(2,1)S(1)} %get-tuple-element.16), channel_id=1, source_target_pairs={{0,30},{2,0},{4,2},{6,4},{8,6},{10,8},{12,10},{14,12},{16,14},{18,... | collective-permute-start | bytes 196616 | tf_op jit(solution)/shard_map/ppermute | solution.py:185
  196.6 59.6 %all-to-all-start.1 = ((bf16[16,8,2048]{2,1,0:T(8,128)(2,1)}), bf16[16,8,2048]{2,1,0:T(8,128)(2,1)S(1)}, u32[]{:S(2)}, u32[]{:S(2)}) async-start(bf16[16,8,2048]{2,1,0:T(8,128)(2,1)} %convolution_convert_fusion), calls=%async_computation.2 | async-start | bytes 1048576 | tf_op jit(solution)/shard_map/all_to_all | solution.py:155
  200.2 74.1 %reduce-scatter.6.cloned.1.call-start = ((), (), s32[]{:S(2)}) async-start(), calls=%async_computation.9 | async-start | bytes 786432 | tf_op jit(solution)/shard_map/reduce_scatter | solution.py:160
  200.2 16.0 %collective-permute-start.2 = (bf16[16,2048]{1,0:T(8,128)(2,1)S(1)}, bf16[16,2048]{1,0:T(8,128)(2,1)S(1)}, u32[]{:S(2)}, u32[]{:S(2)}) collective-permute-start(bf16[16,2048]{1,0:T(8,128)(2,1)S(1)} %collective-permute-done), channel_id=1, source_target_pairs={{0,2},{2,4},{4,6},{6,8},{8,10},{10,12},{12,14},{14,16},{16,18},{18... | collective-permute-start | bytes 196616 | tf_op jit(solution)/shard_map/ppermute | solution.py:180
  202.1 14.1 %collective-permute-start.3 = (bf16[16,2048]{1,0:T(8,128)(2,1)S(1)}, bf16[16,2048]{1,0:T(8,128)(2,1)S(1)}, u32[]{:S(2)}, u32[]{:S(2)}) collective-permute-start(bf16[16,2048]{1,0:T(8,128)(2,1)S(1)} %collective-permute-done.1), channel_id=1, source_target_pairs={{0,30},{2,0},{4,2},{6,4},{8,6},{10,8},{12,10},{14,12},{16,14},{18,... | collective-permute-start | bytes 196616 | tf_op jit(solution)/shard_map/ppermute | solution.py:185
  216.2 7.9 %collective-permute-start.4 = (bf16[16,2048]{1,0:T(8,128)(2,1)S(1)}, bf16[16,2048]{1,0:T(8,128)(2,1)S(1)}, u32[]{:S(2)}, u32[]{:S(2)}) collective-permute-start(bf16[16,2048]{1,0:T(8,128)(2,1)S(1)} %collective-permute-done.2), channel_id=1, source_target_pairs={{0,2},{2,4},{4,6},{6,8},{8,10},{10,12},{12,14},{14,16},{16,18},{18... | collective-permute-start | bytes 196616 | tf_op jit(solution)/shard_map/ppermute | solution.py:180
  216.2 7.9 %collective-permute-start.5 = (bf16[16,2048]{1,0:T(8,128)(2,1)S(1)}, bf16[16,2048]{1,0:T(8,128)(2,1)S(1)}, u32[]{:S(2)}, u32[]{:S(2)}) collective-permute-start(bf16[16,2048]{1,0:T(8,128)(2,1)S(1)} %collective-permute-done.3), channel_id=1, source_target_pairs={{0,30},{2,0},{4,2},{6,4},{8,6},{10,8},{12,10},{14,12},{16,14},{18,... | collective-permute-start | bytes 196616 | tf_op jit(solution)/shard_map/ppermute | solution.py:185
  224.1 8.0 %collective-permute-start.6 = (bf16[16,2048]{1,0:T(8,128)(2,1)S(1)}, bf16[16,2048]{1,0:T(8,128)(2,1)S(1)}, u32[]{:S(2)}, u32[]{:S(2)}) collective-permute-start(bf16[16,2048]{1,0:T(8,128)(2,1)S(1)} %collective-permute-done.4), channel_id=1, source_target_pairs={{0,2},{2,4},{4,6},{6,8},{8,10},{10,12},{12,14},{14,16},{16,18},{18... | collective-permute-start | bytes 196616 | tf_op jit(solution)/shard_map/ppermute | solution.py:180
  224.1 8.0 %collective-permute-start.7 = (bf16[16,2048]{1,0:T(8,128)(2,1)S(1)}, bf16[16,2048]{1,0:T(8,128)(2,1)S(1)}, u32[]{:S(2)}, u32[]{:S(2)}) collective-permute-start(bf16[16,2048]{1,0:T(8,128)(2,1)S(1)} %collective-permute-done.5), channel_id=1, source_target_pairs={{0,30},{2,0},{4,2},{6,4},{8,6},{10,8},{12,10},{14,12},{16,14},{18,... | collective-permute-start | bytes 196616 | tf_op jit(solution)/shard_map/ppermute | solution.py:185
  232.0 7.9 %collective-permute-start.8 = (bf16[16,2048]{1,0:T(8,128)(2,1)S(1)}, bf16[16,2048]{1,0:T(8,128)(2,1)S(1)}, u32[]{:S(2)}, u32[]{:S(2)}) collective-permute-start(bf16[16,2048]{1,0:T(8,128)(2,1)S(1)} %collective-permute-done.6), channel_id=1, source_target_pairs={{0,2},{2,4},{4,6},{6,8},{8,10},{10,12},{12,14},{14,16},{16,18},{18... | collective-permute-start | bytes 196616 | tf_op jit(solution)/shard_map/ppermute | solution.py:180
  232.0 7.9 %collective-permute-start.9 = (bf16[16,2048]{1,0:T(8,128)(2,1)S(1)}, bf16[16,2048]{1,0:T(8,128)(2,1)S(1)}, u32[]{:S(2)}, u32[]{:S(2)}) collective-permute-start(bf16[16,2048]{1,0:T(8,128)(2,1)S(1)} %collective-permute-done.7), channel_id=1, source_target_pairs={{0,30},{2,0},{4,2},{6,4},{8,6},{10,8},{12,10},{14,12},{16,14},{18,... | collective-permute-start | bytes 196616 | tf_op jit(solution)/shard_map/ppermute | solution.py:185
  239.9 7.9 %collective-permute-start.10 = (bf16[16,2048]{1,0:T(8,128)(2,1)S(1)}, bf16[16,2048]{1,0:T(8,128)(2,1)S(1)}, u32[]{:S(2)}, u32[]{:S(2)}) collective-permute-start(bf16[16,2048]{1,0:T(8,128)(2,1)S(1)} %collective-permute-done.8), channel_id=1, source_target_pairs={{0,2},{2,4},{4,6},{6,8},{8,10},{10,12},{12,14},{14,16},{16,18},{18... | collective-permute-start | bytes 196616 | tf_op jit(solution)/shard_map/ppermute | solution.py:180
  239.9 7.9 %collective-permute-start.11 = (bf16[16,2048]{1,0:T(8,128)(2,1)S(1)}, bf16[16,2048]{1,0:T(8,128)(2,1)S(1)}, u32[]{:S(2)}, u32[]{:S(2)}) collective-permute-start(bf16[16,2048]{1,0:T(8,128)(2,1)S(1)} %collective-permute-done.9), channel_id=1, source_target_pairs={{0,30},{2,0},{4,2},{6,4},{8,6},{10,8},{12,10},{14,12},{16,14},{18,... | collective-permute-start | bytes 196616 | tf_op jit(solution)/shard_map/ppermute | solution.py:185
  247.7 8.4 %collective-permute-start.12 = (bf16[16,2048]{1,0:T(8,128)(2,1)S(1)}, bf16[16,2048]{1,0:T(8,128)(2,1)S(1)}, u32[]{:S(2)}, u32[]{:S(2)}) collective-permute-start(bf16[16,2048]{1,0:T(8,128)(2,1)S(1)} %collective-permute-done.10), channel_id=1, source_target_pairs={{0,2},{2,4},{4,6},{6,8},{8,10},{10,12},{12,14},{14,16},{16,18},{18... | collective-permute-start | bytes 196616 | tf_op jit(solution)/shard_map/ppermute | solution.py:180
  247.8 8.4 %collective-permute-start.13 = (bf16[16,2048]{1,0:T(8,128)(2,1)S(1)}, bf16[16,2048]{1,0:T(8,128)(2,1)S(1)}, u32[]{:S(2)}, u32[]{:S(2)}) collective-permute-start(bf16[16,2048]{1,0:T(8,128)(2,1)S(1)} %collective-permute-done.11), channel_id=1, source_target_pairs={{0,30},{2,0},{4,2},{6,4},{8,6},{10,8},{12,10},{14,12},{16,14},{18,... | collective-permute-start | bytes 196616 | tf_op jit(solution)/shard_map/ppermute | solution.py:185
  256.1 8.8 %collective-permute-start.14 = (bf16[16,2048]{1,0:T(8,128)(2,1)S(1)}, bf16[16,2048]{1,0:T(8,128)(2,1)S(1)}, u32[]{:S(2)}, u32[]{:S(2)}) collective-permute-start(bf16[16,2048]{1,0:T(8,128)(2,1)S(1)} %collective-permute-done.12), channel_id=1, source_target_pairs={{0,2},{2,4},{4,6},{6,8},{8,10},{10,12},{12,14},{14,16},{16,18},{18... | collective-permute-start | bytes 196616 | tf_op jit(solution)/shard_map/ppermute | solution.py:180
  259.1 6.3 %copy-start.11 = (bf16[128,2048]{1,0:T(8,128)(2,1)S(1)}, bf16[128,2048]{1,0:T(8,128)(2,1)}, u32[]{:S(2)}) copy-start(bf16[128,2048]{1,0:T(8,128)(2,1)} %param.43) | copy-start | bytes 1572868
  264.9 151.4 %reduce-scatter.8.cloned.1.call-start = ((), (), s32[]{:S(2)}) async-start(), calls=%async_computation.10 | async-start | bytes 2162688 | tf_op jit(solution)/shard_map/reduce_scatter | solution.py:196
  264.9 16.1 %copy-start.9 = (f32[16,4]{0,1:T(4,128)S(1)}, f32[16,4]{0,1:T(4,128)}, u32[]{:S(2)}) copy-start(f32[16,4]{0,1:T(4,128)} %param.38) | copy-start | bytes 772
  274.3 17.8 %all-to-all-start.2 = ((bf16[16,8,1024]{2,1,0:T(8,128)(2,1)}), bf16[16,8,1024]{2,1,0:T(8,128)(2,1)S(1)}, u32[]{:S(2)}, u32[]{:S(2)}) async-start(bf16[16,8,1024]{2,1,0:T(8,128)(2,1)} %bitcast.96), calls=%async_computation.4 | async-start | bytes 524288 | tf_op jit(solution)/shard_map/all_to_all | solution.py:163
  (3 other events, 6.5 us)
Sparse Core Ops, SparseCore 0:
  27.6 78.4 reduce-scatter.3
  108.8 60.2 all-gather.1
  171.9 15.9 all-reduce.1
  265.0 9.3 reduce-scatter.5
  276.4 139.7 reduce-scatter.7
